TPU v7x, 32 devices: a whole 2x2x4 slice. The times are simulated.
32 devices in a mesh: row: 8 (over z, y), col: 4 (over x, core).
Axes of the slice: x: 2, y: 2, z: 4, core: 2. Of those that a mesh axis runs over, the one named last changes fastest.
Arguments:
- tokens: bfloat16 [4096, 2048], P('row'), may hold values from -6 to 6
- outer_weight: bfloat16 [2048, 1024], P(None, 'col'), may hold values from -0.125 to 0.125
- inner_weight: bfloat16 [2048, 1024], P(None, 'col'), may hold values from -0.125 to 0.125
- value_weight: bfloat16 [2048, 1024], P(None, 'col'), may hold values from -0.125 to 0.125
- conv_taps: float32 [3, 3, 1024], P(None, None, 'col'), may hold values from -3.5 to 3.5
- feature_weight: float32 [33, 128], replicated, may hold values from -1 to 1
- feature_phase: float32 [128], replicated, may hold values from -3.140625 to 3.140625
- inner_mats: float32 [2, 128, 128], replicated, may hold values from -0.5 to 0.5
- inner_phase: float32 [2, 128], replicated, may hold values from -3.140625 to 3.140625
- frequency: float32 [128], replicated, may hold values from 0.1 to 1.9
- forward_weight: float32 [128, 1024], P(None, 'col'), may hold values from -0.5 to 0.5
- backward_weight: float32 [128, 1024], P(None, 'col'), may hold values from -0.5 to 0.5
- decay_rate: float32 [1024], P('col'), may hold values from 0.2 to 409.6, as said below
- skip_gain: float32 [1024], P('col'), may hold values from -6 to 6
- output_weight: bfloat16 [1024, 2048], replicated, may hold values from -0.1875 to 0.1875
Outputs:
- layer_out: bfloat16 [4096, 2048], P(('row', 'col'))
Inputs may be any that keep to these rules, and one draw needn't show every extreme that they name: `decay_rate`: positive rates of the channels' filter windows.
All inputs are finite; a program needn't handle non-finite values.
Results may differ from a plain program's by a relative error of at most 0.014.
Values may be sent and summed in bfloat16 or wider, within the bound.
A program may use at most 64 MiB of HBM per device.

v0:
```python
import functools
import math

import jax
import jax.numpy as jnp
import numpy as np
from jax import lax
from jax.experimental import pallas as pl
from jax.experimental.pallas import tpu as pltpu
from jax.sharding import PartitionSpec as P

BANDS = 16
INNER = 2
FACTOR = 256


PRECISE = lax.Precision.HIGHEST


def with_halo(array, sides, width):
    for axis, dim in sides:
        devices, length = (lax.axis_size(axis), array.shape[dim])
        up = [(i, (i + 1) % devices) for i in range(devices - 1)]
        down = [(j, i) for i, j in up]
        last = lax.slice_in_dim(array, length - width, length, axis=dim)
        leading = lax.slice_in_dim(array, 0, width, axis=dim)
        before = lax.ppermute(last, axis, up)
        after = lax.ppermute(leading, axis, down)
        array = jnp.concatenate([before, array, after], axis=dim)
    return array


def phases(height, breadth, period):
    row_index = lax.broadcasted_iota(jnp.int32, (height, breadth), 0)
    col_index = lax.broadcasted_iota(jnp.int32, (height, breadth), 1)
    phase_angle = 2.0 * math.pi / period * (row_index * col_index % period).astype(jnp.float32)
    return (jnp.cos(phase_angle), jnp.sin(phase_angle))


def along_last(operand, matrix):
    return jnp.einsum("ckb,bj->ckj", operand, matrix, precision=PRECISE)


def forward_transform(operand, tables):
    cosine_one, sine_one, twist_cos, twist_sin, cosine_two, sine_two = tables
    used_rows = operand.shape[1]
    first_real = jnp.einsum("kr,crb->ckb", cosine_one[:, :used_rows], operand, precision=PRECISE)
    first_imag = -jnp.einsum("kr,crb->ckb", sine_one[:, :used_rows], operand, precision=PRECISE)
    turned_real = first_real * twist_cos + first_imag * twist_sin
    turned_imag = first_imag * twist_cos - first_real * twist_sin
    spec_real = along_last(turned_real, cosine_two) + along_last(turned_imag, sine_two)
    spec_imag = along_last(turned_imag, cosine_two) - along_last(turned_real, sine_two)
    return (spec_real, spec_imag)


def inverse_transform(spec_real, spec_imag, tables, kept_rows):
    cosine_one, sine_one, twist_cos, twist_sin, cosine_two, sine_two = tables
    back_real = along_last(spec_real, cosine_two) - along_last(spec_imag, sine_two)
    back_imag = along_last(spec_imag, cosine_two) + along_last(spec_real, sine_two)
    untwist_real = back_real * twist_cos - back_imag * twist_sin
    untwist_imag = back_imag * twist_cos + back_real * twist_sin
    return jnp.einsum(
        "nk,ckb->cnb", cosine_one[:kept_rows], untwist_real, precision=PRECISE
    ) - jnp.einsum("nk,ckb->cnb", sine_one[:kept_rows], untwist_imag, precision=PRECISE)


def position_filters(
    places,
    seq_length,
    feature_weight,
    feature_phase,
    inner_mats,
    inner_phase,
    frequency,
    forward_cols,
    backward_cols,
    rates,
):
    scaled = places.astype(jnp.float32) / (seq_length - 1)
    band_ints = 1 + jnp.arange(BANDS, dtype=jnp.int32) * (seq_length // (4 * BANDS))
    turns = places[:, None] * band_ints[None, :] % seq_length
    angles = 2.0 * math.pi / seq_length * turns.astype(jnp.float32)
    features = jnp.concatenate([scaled[:, None], jnp.cos(angles), -jnp.sin(angles)], axis=1)
    hidden = jnp.sin(
        frequency * (jnp.dot(features, feature_weight, precision=PRECISE) + feature_phase)
    )
    for level_index in range(INNER):
        hidden = jnp.sin(
            frequency
            * (
                jnp.dot(hidden, inner_mats[level_index], precision=PRECISE)
                + inner_phase[level_index]
            )
        )
    window = jnp.exp(-scaled[:, None] * rates[None, :])
    filter_ahead = jnp.dot(hidden, forward_cols, precision=PRECISE) * window
    filter_behind = jnp.dot(hidden, backward_cols, precision=PRECISE) * window
    return (filter_ahead, filter_behind)


def on_device(
    tokens,
    outer_weight,
    inner_weight,
    value_weight,
    conv_taps,
    feature_weight,
    feature_phase,
    inner_mats,
    inner_phase,
    frequency,
    forward_weight,
    backward_weight,
    decay_rate,
    skip_gain,
    output_weight,
):
    block_rows = tokens.shape[0]
    seq_length = block_rows * lax.axis_size("row")
    own_width = outer_weight.shape[1]
    outer_proj = jnp.dot(tokens, outer_weight, preferred_element_type=jnp.float32).astype(
        jnp.bfloat16
    )
    inner_proj = jnp.dot(tokens, inner_weight, preferred_element_type=jnp.float32).astype(
        jnp.bfloat16
    )
    value_proj = jnp.dot(tokens, value_weight, preferred_element_type=jnp.float32).astype(
        jnp.bfloat16
    )
    stacked = jnp.concatenate([outer_proj, inner_proj, value_proj], axis=1)
    padded = with_halo(stacked, (("row", 0),), 1).astype(jnp.float32)
    tap_table = conv_taps.reshape(3, 3 * own_width)
    convolved = padded[:-2] * tap_table[0] + padded[1:-1] * tap_table[1] + padded[2:] * tap_table[2]
    gate_part = convolved[:, :own_width].astype(jnp.bfloat16)
    signal = (convolved[:, own_width : 2 * own_width] * convolved[:, 2 * own_width :]).astype(
        jnp.bfloat16
    )
    offset = lax.axis_index("row") * block_rows
    places = offset + jnp.arange(block_rows, dtype=jnp.int32)
    filter_ahead, filter_behind = position_filters(
        places,
        seq_length,
        feature_weight,
        feature_phase,
        inner_mats,
        inner_phase,
        frequency,
        forward_weight,
        backward_weight,
        decay_rate,
    )
    moved_signal, moved_ahead, moved_behind = (
        lax.all_to_all(signal.astype(jnp.float32), "row", split_axis=1, concat_axis=0, tiled=True),
        lax.all_to_all(filter_ahead, "row", split_axis=1, concat_axis=0, tiled=True),
        lax.all_to_all(filter_behind, "row", split_axis=1, concat_axis=0, tiled=True),
    )
    per_device = moved_ahead.shape[1]
    ahead_rows = moved_ahead.T
    behind_rows = moved_behind.T
    norm_scale = lax.rsqrt(
        1.0
        + jnp.sum(jnp.square(ahead_rows), axis=1)
        + jnp.sum(jnp.square(behind_rows[:, 1:]), axis=1)
    )
    kernel_rows = (
        jnp.concatenate(
            [ahead_rows, jnp.zeros((per_device, 1), jnp.float32), jnp.flip(behind_rows[:, 1:], 1)],
            axis=1,
        )
        * norm_scale[:, None]
    )
    padded_length = 2 * seq_length
    height = padded_length // FACTOR
    tables = (
        phases(height, height, height)
        + phases(height, FACTOR, padded_length)
        + phases(FACTOR, FACTOR, FACTOR)
    )
    kernel_real, kernel_imag = forward_transform(
        kernel_rows.reshape(per_device, height, FACTOR), tables
    )
    signal_real, signal_imag = forward_transform(
        moved_signal.T.reshape(per_device, height // 2, FACTOR), tables
    )
    prod_real = signal_real * kernel_real - signal_imag * kernel_imag
    prod_imag = signal_real * kernel_imag + signal_imag * kernel_real
    response = inverse_transform(prod_real, prod_imag, tables, height // 2) / padded_length
    response = response.reshape(per_device, seq_length).T.astype(jnp.bfloat16)
    returned = lax.all_to_all(response, "row", split_axis=0, concat_axis=1, tiled=True)
    mixed_rows = (
        gate_part.astype(jnp.float32)
        * (returned.astype(jnp.float32) + skip_gain * signal.astype(jnp.float32))
    ).astype(jnp.bfloat16)
    whole_rows = lax.all_to_all(mixed_rows, "col", split_axis=0, concat_axis=1, tiled=True)
    return jnp.dot(whole_rows, output_weight, preferred_element_type=jnp.float32).astype(
        jnp.bfloat16
    )


WIDE = 256


def feature_table(seq_length):
    places = np.arange(seq_length, dtype=np.int64)
    bands = 1 + np.arange(BANDS, dtype=np.int64) * (seq_length // (4 * BANDS))
    angles = 2.0 * np.pi / seq_length * (places[:, None] * bands[None, :] % seq_length)
    scaled = places / (seq_length - 1)
    feats = np.concatenate([scaled[:, None], np.cos(angles), -np.sin(angles)], 1).astype(np.float32)
    high = feats.astype(jnp.bfloat16)
    low = (feats - high.astype(np.float32)).astype(jnp.bfloat16)
    used = np.zeros((seq_length, 128), jnp.bfloat16)
    count = feats.shape[1]
    for start, part in ((0, high), (40, low), (80, high)):
        used[:, start : start + count] = part
    used[:, 120:122] = 1
    return used


def sine_coefficients():
    u = 0.5 * np.cos(np.pi * (np.arange(4000) + 0.5) / 8000)
    powers = np.stack([u ** (2 * i + 1) for i in range(6)], 1)
    return [float(v) for v in np.linalg.lstsq(powers, np.sin(2 * np.pi * u), rcond=None)[0]]


SINE = sine_coefficients()
MAGIC = 12582912.0


def sine_of_turns(turns):
    u = turns - ((turns + MAGIC) - MAGIC)
    square = u * u
    total = SINE[-1]
    for value in SINE[-2::-1]:
        total = total * square + value
    return u * total


def split_two(value):
    high = value.astype(jnp.bfloat16)
    return high, (value - high.astype(jnp.float32)).astype(jnp.bfloat16)


def combine(terms):
    total = None
    for coef, array in terms:
        if abs(coef) < 1e-9:
            continue
        if abs(abs(coef) - 1.0) < 1e-9:
            if total is None:
                total = array if coef > 0 else -array
            else:
                total = total + array if coef > 0 else total - array
        else:
            total = array * coef if total is None else total + array * coef
    return total


def first_stage(planes):
    half = len(planes)
    full, mid = 2 * half, half // 2
    quarter = mid // 2
    theta = 2 * math.pi / full
    add = {r: planes[r] + planes[half - r] for r in range(1, mid)}
    sub = {r: planes[r] - planes[half - r] for r in range(1, mid)}
    add_add = {r: add[r] + add[mid - r] for r in range(1, quarter)}
    add_sub = {r: add[r] - add[mid - r] for r in range(1, quarter)}
    sub_add = {r: sub[r] + sub[mid - r] for r in range(1, quarter)}
    sub_sub = {r: sub[r] - sub[mid - r] for r in range(1, quarter)}
    ends = (planes[0] + planes[mid], planes[0] - planes[mid])
    out = []
    for k in range(half + 1):
        cos = lambda r: math.cos(theta * r * k)
        sin = lambda r: math.sin(theta * r * k)
        if k % 4 == 0:
            real = combine([(1.0, ends[0]), (cos(quarter), add[quarter])] + [(cos(r), add_add[r]) for r in add_add])
            imag = combine([(-sin(r), sub_sub[r]) for r in sub_sub])
        elif k % 2 == 0:
            real = combine([(1.0, ends[1])] + [(cos(r), add_sub[r]) for r in add_sub])
            imag = combine([(-sin(quarter), sub[quarter])] + [(-sin(r), sub_add[r]) for r in sub_add])
        else:
            real = combine([(1.0, planes[0])] + [(cos(r), sub[r]) for r in sub])
            imag = combine([(-sin(mid), planes[mid])] + [(-sin(r), add[r]) for r in add])
        out.append((real, imag))
    return out


def last_stage(pairs):
    half = len(pairs) - 1
    full, mid = 2 * half, half // 2
    quarter = mid // 2
    theta = 2 * math.pi / full
    four = range(0, half + 1, 4)
    two = range(2, half + 1, 4)
    odd = range(1, half + 1, 2)
    real = [p[0] for p in pairs]
    imag = [p[1] for p in pairs]
    out = [None] * half

    def cosines(r, ks):
        return combine([(math.cos(theta * r * k), real[k]) for k in ks])

    def sines(r, ks):
        return combine([(math.sin(theta * r * k), imag[k]) for k in ks])

    out[0] = combine([(1.0, v) for v in real])
    out[mid] = cosines(mid, list(four) + list(two)) - sines(mid, odd)

    def place(r, cos_even, sin_even):
        cos_odd, sin_odd = cosines(r, odd), sines(r, odd)
        out[r] = (cos_even - sin_even) + (cos_odd - sin_odd)
        out[half - r] = (cos_even + sin_even) - (cos_odd + sin_odd)

    for r in range(1, quarter):
        c0, c2, s0, s2 = cosines(r, four), cosines(r, two), sines(r, four), sines(r, two)
        place(r, c0 + c2, s0 + s2)
        place(mid - r, c0 - c2, s2 - s0)
    place(quarter, cosines(quarter, four), sines(quarter, two))
    return out


def tiles(count, body):
    lanes = WIDE // 128

    def one(i, carry):
        body(pl.multiple_of(i // lanes * 16, 16), pl.multiple_of(i % lanes * 128, 128))
        return carry

    lax.fori_loop(0, count // 16 * lanes, one, 0)


def layer_kernel(
    tokens_h, outer_h, inner_h, value_h, feats_h,
    taps, feature_weight, feature_phase, inner_mats, inner_phase, frequency, forward, backward, rate, skip,
    twist_c, twist_s, cos_t, sin_t,
    out_ref,
    tok, weights, feats, hid, sig_send, sig_recv, resp_send, resp_recv, mix_send, mix_recv,
    sums, diffs, turned, filt, back, scale_ref, first_ref, chan, rate_col, energy_ref, gate_ref, signal_ref,
    local_sem, edge_send, edge_recv, hid_s, hid_r, sig_s, sig_r, resp_s, resp_r, mix_s, mix_r,
):
    f32, bf16 = jnp.float32, jnp.bfloat16
    dot = functools.partial(jnp.dot, preferred_element_type=f32)
    n_row, n_col = lax.axis_size("row"), lax.axis_size("col")
    row, col = lax.axis_index("row"), lax.axis_index("col")
    length, rows = feats_h.shape[0], tokens_h.shape[0]
    quarter = length // n_col
    width = outer_h.shape[1]
    count = width // n_row
    planes = length // WIDE
    per = rows // WIDE
    mesh_id = pl.DeviceIdType.MESH

    barrier = pltpu.get_barrier_semaphore()
    for o in range(1, n_row):
        pl.semaphore_signal(barrier, inc=1, device_id=(lax.rem(row + o, n_row), col), device_id_type=mesh_id)
    for o in range(1, n_col):
        pl.semaphore_signal(barrier, inc=1, device_id=(row, lax.rem(col + o, n_col)), device_id_type=mesh_id)
    loads = [
        pltpu.make_async_copy(
            feats_h.at[pl.ds(pl.multiple_of(col * quarter, 512), quarter)], feats, local_sem.at[0]),
        pltpu.make_async_copy(tokens_h, tok.at[pl.ds(0, rows)], local_sem.at[1]),
        pltpu.make_async_copy(inner_h, weights.at[1], local_sem.at[2]),
        pltpu.make_async_copy(value_h, weights.at[2], local_sem.at[3]),
        pltpu.make_async_copy(outer_h, weights.at[0], local_sem.at[4]),
    ]
    for load in loads:
        load.start()

    turn = frequency[...] * (0.5 / math.pi)
    high, low = split_two(feature_weight[...] * turn)
    phase_high, phase_low = split_two(feature_phase[...] * turn)
    used = high.shape[0]
    first_ref[...] = jnp.zeros_like(first_ref)
    first_ref[0:used] = high.astype(f32)
    first_ref[40 : 40 + used] = high.astype(f32)
    first_ref[80 : 80 + used] = low.astype(f32)
    first_ref[120:121] = phase_high.astype(f32)
    first_ref[121:122] = phase_low.astype(f32)
    first_w = first_ref[...].astype(bf16)
    inner_w = []
    for level in range(INNER):
        mat_high, mat_low = split_two(inner_mats[level] * turn)
        inner_w.append(jnp.concatenate([
            jnp.concatenate([mat_high, mat_low], 1), jnp.concatenate([mat_high, jnp.zeros_like(mat_low)], 1)], 0))
    inner_p = inner_phase[...] * turn
    chan[0] = forward[...].T
    chan[1] = backward[...].T
    rate_col[...] = jnp.broadcast_to(rate[...], (128, width)).T
    own = pl.ds(pl.multiple_of(row * count, 16), count)
    both_w = jnp.concatenate([chan[0, own, :], chan[1, own, :]], 0).astype(bf16)
    rates = rate_col[own, 0:1]
    chunk = 512
    energy_ref[...] = jnp.zeros_like(energy_ref)

    def hidden_chunk(i):
        at = pl.ds(i * chunk, chunk)
        hidden = sine_of_turns(dot(feats[at, :], first_w))
        for level in range(INNER):
            h_high, h_low = split_two(hidden)
            wide = dot(jnp.concatenate([h_high, h_low], 1), inner_w[level])
            hidden = sine_of_turns(wide[:, :128] + wide[:, 128:] + inner_p[level : level + 1, :])
        hid[col, at, :] = hidden.astype(bf16)

    def filter_chunk(owner, i):
        at = pl.ds(pl.multiple_of(owner * quarter + i * chunk, chunk), chunk)
        both = lax.dot_general(both_w, hid[owner, pl.ds(i * chunk, chunk), :], (((1,), (1,)), ((), ())),
                               preferred_element_type=f32)
        place = lax.broadcasted_iota(jnp.int32, (count, chunk), 1) + (owner * quarter + i * chunk)
        window = jnp.exp(place.astype(f32) * (-1.0 / (length - 1)) * rates)
        ahead = both[:count] * window
        behind = jnp.where(place == 0, 0.0, both[count:] * window)
        sums[:, at] = ahead + behind
        diffs[:, at] = ahead - behind
        energy_ref[...] += jnp.broadcast_to(
            jnp.sum(ahead * ahead + behind * behind, axis=1, keepdims=True), (count, 128))

    pieces = quarter // chunk
    partner = col + 1 - 2 * lax.rem(col, 2)
    across = lax.rem(col + 2, n_col)

    def pass_on(kind, owner, i, target):
        part = hid.at[owner, pl.ds(i * chunk, chunk)]
        return pltpu.make_async_remote_copy(
            src_ref=part, dst_ref=part, send_sem=hid_s.at[kind, i], recv_sem=hid_r.at[kind, i],
            device_id=(row, target), device_id_type=mesh_id)

    loads[0].wait()
    for i in range(pieces):
        hidden_chunk(i)

    pl.semaphore_wait(barrier, n_row + n_col - 2)
    edges = [
        pltpu.make_async_remote_copy(
            src_ref=tokens_h.at[pl.ds(rows - 16 if i == 0 else 0, 16)],
            dst_ref=tok.at[pl.ds(rows + 16 * i, 16)],
            send_sem=edge_send.at[i], recv_sem=edge_recv.at[i],
            device_id=(lax.rem(row + (1 if i == 0 else n_row - 1), n_row), col), device_id_type=mesh_id)
        for i in range(2)
    ]
    for edge in edges:
        edge.start()
    to_across = [pass_on(0, col, i, across) for i in range(pieces)]
    to_partner = [pass_on(1, col, i, partner) for i in range(pieces)]
    relayed = [pass_on(2, across, i, partner) for i in range(pieces)]
    for copy in to_across + to_partner:
        copy.start()
    loads[1].wait()
    loads[2].wait()
    loads[3].wait()
    for edge in edges:
        edge.wait()

    index = lax.broadcasted_iota(jnp.int32, (rows, width), 0)
    has_before = jnp.where(row > 0, 1.0, 0.0)
    has_after = jnp.where(row < n_row - 1, 1.0, 0.0)

    def convolved(j):
        proj = dot(tok[...], weights[j]).astype(bf16).astype(f32)
        main = proj[:rows]
        first = proj[rows + 15 : rows + 16] * has_before
        last = proj[rows + 16 : rows + 17] * has_after
        before = jnp.where(index == 0, first, pltpu.roll(main, 1, 0))
        after = jnp.where(index == rows - 1, last, pltpu.roll(main, rows - 1, 0))
        return before * taps[0, j : j + 1, :] + main * taps[1, j : j + 1, :] + after * taps[2, j : j + 1, :]

    signal = (convolved(1) * convolved(2)).astype(bf16)
    signal_ref[...] = signal
    flipped = signal.astype(f32).T.astype(bf16)
    for g in range(n_row):
        sig_send[g] = flipped[g * count : (g + 1) * count]

    def exchange(send, recv, s_sem, r_sem, size, me, target):
        copies = []
        for o in range(1, size):
            peer = lax.rem(me + o, size)
            copies.append(pltpu.make_async_remote_copy(
                src_ref=send.at[peer], dst_ref=recv.at[me],
                send_sem=s_sem.at[o], recv_sem=r_sem.at[o], device_id=target(peer), device_id_type=mesh_id))
        for copy in copies:
            copy.start()
        recv[me] = send[me]
        return copies

    along_row = lambda peer: (peer, col)
    along_col = lambda peer: (row, peer)
    travelling = exchange(sig_send, sig_recv, sig_s, sig_r, n_row, row, along_row)

    loads[4].wait()
    gate_ref[...] = convolved(0).astype(bf16)
    for i in range(pieces):
        filter_chunk(col, i)
    for i in range(pieces):
        to_partner[i].wait()
        filter_chunk(partner, i)
    for i in range(pieces):
        to_across[i].wait()
        relayed[i].start()
    for i in range(pieces):
        filter_chunk(across, i)
    for i in range(pieces):
        relayed[i].wait()
        filter_chunk(lax.rem(partner + 2, n_col), i)
    scale_ref[...] = lax.rsqrt(1.0 + energy_ref[...]) * (0.5 / length)

    def turn_into(first, pairs, top, left, weighted):
        for k, (real, imag) in enumerate(pairs):
            c, s = twist_c[k : k + 1, pl.ds(left, 128)], twist_s[k : k + 1, pl.ds(left, 128)]
            if weighted and k not in (0, planes):
                c, s = c * 2.0, s * 2.0
            at = pl.ds(pl.multiple_of(k * count + top, 16), 16)
            if imag is None:
                new_real, new_imag = real * c, -(real * s)
            else:
                new_real, new_imag = real * c + imag * s, imag * c - real * s
            turned[first, at, pl.ds(left, 128)] = new_real.astype(bf16)
            turned[first + 1, at, pl.ds(left, 128)] = new_imag.astype(bf16)

    def filter_tile(top, left):
        scale = scale_ref[pl.ds(top, 16), :]
        for which, source in enumerate((sums, diffs)):
            got = [source[pl.ds(top, 16), pl.ds(pl.multiple_of(r * WIDE + left, 128), 128)] * scale for r in range(planes)]
            turn_into(2 * which, first_stage(got), top, left, True)

    tiles(count, filter_tile)
    filt[0] = dot(turned[0], cos_t[...]) + dot(turned[1], sin_t[...])
    filt[1] = dot(turned[3], cos_t[...]) - dot(turned[2], sin_t[...])
    for copy in travelling:
        copy.wait()

    def signal_tile(top, left):
        got = [sig_recv[r // per, pl.ds(top, 16), pl.ds(pl.multiple_of(r % per * WIDE + left, 128), 128)].astype(f32)
               for r in range(planes)]
        turn_into(0, first_stage(got), top, left, False)

    tiles(count, signal_tile)
    real = dot(turned[0], cos_t[...]) + dot(turned[1], sin_t[...])
    imag = dot(turned[1], cos_t[...]) - dot(turned[0], sin_t[...])
    prod_real = (real * filt[0] - imag * filt[1]).astype(bf16)
    prod_imag = (real * filt[1] + imag * filt[0]).astype(bf16)
    back[0] = dot(prod_real, cos_t[...]) - dot(prod_imag, sin_t[...])
    back[1] = dot(prod_imag, cos_t[...]) + dot(prod_real, sin_t[...])

    def back_tile(top, left):
        pairs = []
        for k in range(planes + 1):
            c, s = twist_c[k : k + 1, pl.ds(left, 128)], twist_s[k : k + 1, pl.ds(left, 128)]
            at = pl.ds(pl.multiple_of(k * count + top, 16), 16)
            b_real, b_imag = back[0, at, pl.ds(left, 128)], back[1, at, pl.ds(left, 128)]
            pairs.append((b_real * c - b_imag * s, b_imag * c + b_real * s))
        for r, plane in enumerate(last_stage(pairs)):
            at = pl.multiple_of(r % per * WIDE + left, 128)
            resp_send[r // per, pl.ds(top, 16), pl.ds(at, 128)] = plane.astype(bf16)

    tiles(count, back_tile)
    for copy in exchange(resp_send, resp_recv, resp_s, resp_r, n_row, row, along_row):
        copy.wait()
    response = jnp.concatenate([resp_recv[g].astype(f32) for g in range(n_row)], 0).T
    mixed = (gate_ref[...].astype(f32) * (response + skip[...] * signal_ref[...].astype(f32))).astype(bf16)
    share = rows // n_col
    for p in range(n_col):
        mix_send[p] = mixed[p * share : (p + 1) * share]
    travelling = exchange(mix_send, mix_recv, mix_s, mix_r, n_col, col, along_col)
    for copy in travelling:
        copy.wait()
    for p in range(n_col):
        out_ref[:, p * width : (p + 1) * width] = mix_recv[p]


def fits(tokens_rows, seq_length, own_width, row_devices, col_devices, units):
    planes = seq_length // WIDE
    members = own_width // row_devices
    return (
        own_width % 128 == 0
        and members % 16 == 0
        and tokens_rows % WIDE == 0
        and seq_length % 512 == 0
        and planes % 8 == 0
        and 8 <= planes <= 32
        and units == 128
        and tokens_rows % 64 == 0
        and col_devices == 4
        and seq_length % 2048 == 0
    )


def on_device_fast(
    tokens, outer_weight, inner_weight, value_weight, conv_taps, feature_weight, feature_phase,
    inner_mats, inner_phase, frequency, forward_weight, backward_weight, decay_rate, skip_gain, output_weight,
):
    f32, bf16 = jnp.float32, jnp.bfloat16
    rows, depth = tokens.shape
    devices = lax.axis_size("row")
    seq_length = rows * devices
    width = outer_weight.shape[1]
    members = width // devices
    planes = seq_length // WIDE
    n_col = lax.axis_size("col")
    k_index = np.arange(planes + 1)[:, None] * np.arange(WIDE)[None, :]
    twist_c = jnp.asarray(np.cos(2 * np.pi * k_index / (2 * seq_length)), f32)
    twist_s = jnp.asarray(np.sin(2 * np.pi * k_index / (2 * seq_length)), f32)
    w_index = np.arange(WIDE)[:, None] * np.arange(WIDE)[None, :] % WIDE
    cos_t = jnp.asarray(np.cos(2 * np.pi * w_index / WIDE), bf16)
    sin_t = jnp.asarray(np.sin(2 * np.pi * w_index / WIDE), bf16)
    spec_rows = (planes + 1) * members
    any_spec = pl.BlockSpec(memory_space=pl.ANY)
    vmem = pl.BlockSpec(memory_space=pltpu.VMEM)
    dma = pltpu.SemaphoreType.DMA
    share = rows // n_col
    pieces = seq_length // n_col // 512
    exchanged = pltpu.VMEM((devices, members, rows), bf16)
    spread = pltpu.VMEM((n_col, share, width), bf16)
    mixed = pl.pallas_call(
        layer_kernel,
        out_shape=jax.ShapeDtypeStruct((share, n_col * width), bf16),
        in_specs=[any_spec] * 5 + [vmem] * 14,
        out_specs=vmem,
        scratch_shapes=[
            pltpu.VMEM((rows + 32, depth), bf16),
            pltpu.VMEM((3, depth, width), bf16),
            pltpu.VMEM((seq_length // n_col, 128), bf16),
            pltpu.VMEM((n_col, seq_length // n_col, 128), bf16),
            exchanged, exchanged, exchanged, exchanged, spread, spread,
            pltpu.VMEM((members, seq_length), f32),
            pltpu.VMEM((members, seq_length), f32),
            pltpu.VMEM((4, spec_rows, WIDE), bf16),
            pltpu.VMEM((2, spec_rows, WIDE), f32),
            pltpu.VMEM((2, spec_rows, WIDE), f32),
            pltpu.VMEM((members, 128), f32),
            pltpu.VMEM((128, 128), f32),
            pltpu.VMEM((2, width, 128), f32),
            pltpu.VMEM((width, 128), f32),
            pltpu.VMEM((members, 128), f32),
            pltpu.VMEM((rows, width), bf16),
            pltpu.VMEM((rows, width), bf16),
            dma((5,)), dma((2,)), dma((2,)), dma((3, pieces)), dma((3, pieces)),
            dma((devices,)), dma((devices,)), dma((devices,)), dma((devices,)), dma((n_col,)), dma((n_col,)),
        ],
        compiler_params=pltpu.CompilerParams(
            collective_id=0, has_side_effects=True, vmem_limit_bytes=GRANT),
        name="layer",
    )(
        tokens, outer_weight, inner_weight, value_weight, jnp.asarray(feature_table(seq_length)),
        conv_taps, feature_weight, feature_phase[None], inner_mats, inner_phase, frequency[None],
        forward_weight, backward_weight, decay_rate[None], skip_gain[None], twist_c, twist_s, cos_t, sin_t,
    )
    return jnp.dot(mixed, output_weight, preferred_element_type=f32).astype(bf16)


GRANT = 54 * 1024 * 1024


def on_any(*args):
    tokens, outer_weight, feature_weight = args[0], args[1], args[5]
    devices = lax.axis_size("row")
    if fits(tokens.shape[0], tokens.shape[0] * devices, outer_weight.shape[1], devices, lax.axis_size("col"), feature_weight.shape[1]):
        return on_device_fast(*args)
    return on_device(*args)


def solution(mesh):
    placed = (
        P("row", None),
        P(None, "col"),
        P(None, "col"),
        P(None, "col"),
        P(None, None, "col"),
        P(),
        P(),
        P(),
        P(),
        P(),
        P(None, "col"),
        P(None, "col"),
        P("col"),
        P("col"),
        P(),
    )
    return jax.shard_map(
        on_any, mesh=mesh, in_specs=placed, out_specs=P(("row", "col"), None), check_vma=False
    )
```

profile of v0, /device:TPU:0, one launch (start us, length us, event | category | flops | bytes accessed | tf_op | source)
XLA Modules:
  0.0 36.4 jit_solution(11296561609518672340)
XLA Ops:
  0.0 0.0 copy-start
  0.0 33.9 %layer.1 = bf16[128,1024]{1,0:T(8,128)(2,1)} custom-call(bf16[512,2048]{1,0:T(8,128)(2,1)} %tokens_h.1, bf16[2048,256]{1,0:T(8,128)(2,1)} %outer_h.1, bf16[2048,256]{1,0:T(8,128)(2,1)} %inner_h.1, bf16[2048,256]{1,0:T(8,128)(2,1)} %value_h.1, bf16[4096,128]{1,0:T(8,128)(2,1)} %constant.14.clone.feats_h, f32[3,3,256]{2,1,0:T(4,128)} %taps.1, ...), custom_call_target="tpu_custom_call" | custom-call | tf_op jit(solution)/shard_map/layer/pallas_call | solution.py:611
  33.9 0.0 copy-done
  33.9 2.5 %convolution_convert_fusion = bf16[128,2048]{1,0:T(8,128)(2,1)} fusion(bf16[128,1024]{1,0:T(8,128)(2,1)} %layer.1, bf16[1024,2048]{1,0:T(8,128)(2,1)S(1)} %copy-done), kind=kOutput, calls=%fused_computation | convolution fusion | flops 537133056 | bytes 4980736 | tf_op jit(solution)/shard_map/dot_general | solution.py:645
Async XLA Ops:
  0.0 33.9 %copy-start = (bf16[1024,2048]{1,0:T(8,128)(2,1)S(1)}, bf16[1024,2048]{1,0:T(8,128)(2,1)}, u32[]{:S(2)}) copy-start(bf16[1024,2048]{1,0:T(8,128)(2,1)} %param.34) | copy-start | bytes 12582916
where the time goes:
time: 36.6 us; the launch traced here: 36.4 us
  Pallas kernels  33.9 us (93%)
  matrix products  2.47 us (7%)
    pallas_call x1, Pallas kernels, on_device_fast(): pl.pallas_call(layer_kernel, out_shape=jax.ShapeDtypeStruct((share, n_col...  33.9 us
    dot_general x1, matrix products, on_device_fast(): jnp.dot(mixed, output_weight, preferred_element_type=f32).astype(bf16)  2.47 us

commit v1 on v0

--- a/solution.py
+++ b/solution.py
@@ -318,35 +318,38 @@
     return out
 
 
-def tiles(count, body):
-    lanes = WIDE // 128
-
-    def one(i, carry):
-        body(pl.multiple_of(i // lanes * 16, 16), pl.multiple_of(i % lanes * 128, 128))
-        return carry
-
-    lax.fori_loop(0, count // 16 * lanes, one, 0)
+GROUP = 16
+LANES = 128
+CHUNK = 512
 
 
 def layer_kernel(
-    tokens_h, outer_h, inner_h, value_h, feats_h,
-    taps, feature_weight, feature_phase, inner_mats, inner_phase, frequency, forward, backward, rate, skip,
-    twist_c, twist_s, cos_t, sin_t,
+    tokens_h, outer_h, inner_h, value_h, feats_h, output_h,
+    taps_h, feature_weight_h, feature_phase_h, inner_mats_h, inner_phase_h, frequency_h, forward_h, backward_h,
+    rate_h, skip_h, twist_h, trig_h,
     out_ref,
-    tok, weights, feats, hid, sig_send, sig_recv, resp_send, resp_recv, mix_send, mix_recv,
-    sums, diffs, turned, filt, back, scale_ref, first_ref, chan, rate_col, energy_ref, gate_ref, signal_ref,
-    local_sem, edge_send, edge_recv, hid_s, hid_r, sig_s, sig_r, resp_s, resp_r, mix_s, mix_r,
+    tok, weights, outer_w, feats, output_w, taps, feature_weight, feature_phase, inner_mats, inner_phase, frequency,
+    forward, backward, rate, skip, twist, trig,
+    hid, sig_send, sig_recv, gs_send, gs_recv, resp_send, resp_recv,
+    sums, diffs, turned, filt, back, scale_ref, first_ref, chan, rate_col, energy_ref, proj_ref, signal_ref, total_ref,
+    edge_ref, edge_out, edge_in, end_ref,
+    load_sem, small_sem, edge_send, edge_recv, hid_s, hid_r, sig_s, sig_r, gs_s, gs_r, resp_s, resp_r,
 ):
     f32, bf16 = jnp.float32, jnp.bfloat16
     dot = functools.partial(jnp.dot, preferred_element_type=f32)
     n_row, n_col = lax.axis_size("row"), lax.axis_size("col")
     row, col = lax.axis_index("row"), lax.axis_index("col")
-    length, rows = feats_h.shape[0], tokens_h.shape[0]
-    quarter = length // n_col
+    rows, depth = tokens_h.shape
+    length = rows * n_row
+    half = feats.shape[0]
     width = outer_h.shape[1]
     count = width // n_row
+    parts = count // GROUP
+    wide = width // parts
     planes = length // WIDE
     per = rows // WIDE
+    share = rows // n_col
+    spec = (planes + 1) * GROUP
     mesh_id = pl.DeviceIdType.MESH
 
     barrier = pltpu.get_barrier_semaphore()
@@ -354,17 +357,47 @@
         pl.semaphore_signal(barrier, inc=1, device_id=(lax.rem(row + o, n_row), col), device_id_type=mesh_id)
     for o in range(1, n_col):
         pl.semaphore_signal(barrier, inc=1, device_id=(row, lax.rem(col + o, n_col)), device_id_type=mesh_id)
-    loads = [
+    side = lax.rem(col, 2)
+    partner = col + 1 - 2 * side
+    small = [
+        pltpu.make_async_copy(source, target, small_sem.at[i])
+        for i, (source, target) in enumerate([
+            (feature_weight_h, feature_weight), (feature_phase_h, feature_phase), (inner_mats_h, inner_mats),
+            (inner_phase_h, inner_phase), (frequency_h, frequency), (forward_h, forward), (backward_h, backward),
+            (rate_h, rate), (taps_h, taps), (skip_h, skip), (twist_h, twist), (trig_h, trig)])
+    ]
+    feature_load = pltpu.make_async_copy(
+        feats_h.at[pl.ds(pl.multiple_of(side * half, CHUNK), half)], feats, load_sem.at[0])
+    first_load = pltpu.make_async_copy(tokens_h.at[0:16], tok.at[0:16], load_sem.at[1])
+    last_load = pltpu.make_async_copy(tokens_h.at[rows - 16 : rows], tok.at[rows - 16 : rows], load_sem.at[2])
+    token_load = pltpu.make_async_copy(tokens_h.at[16 : rows - 16], tok.at[16 : rows - 16], load_sem.at[3])
+    weight_loads = [
+        [
+            pltpu.make_async_copy(
+                source.at[:, h * wide : (h + 1) * wide], weights.at[h, :, j * wide : (j + 1) * wide],
+                load_sem.at[4 + 2 * h + j])
+            for j, source in enumerate((inner_h, value_h))
+        ]
+        for h in range(parts)
+    ]
+    base = 4 + 2 * parts
+    outer_load = pltpu.make_async_copy(outer_h, outer_w, load_sem.at[base])
+    output_loads = [
         pltpu.make_async_copy(
-            feats_h.at[pl.ds(pl.multiple_of(col * quarter, 512), quarter)], feats, local_sem.at[0]),
-        pltpu.make_async_copy(tokens_h, tok.at[pl.ds(0, rows)], local_sem.at[1]),
-        pltpu.make_async_copy(inner_h, weights.at[1], local_sem.at[2]),
-        pltpu.make_async_copy(value_h, weights.at[2], local_sem.at[3]),
-        pltpu.make_async_copy(outer_h, weights.at[0], local_sem.at[4]),
+            output_h.at[c * width + h * wide : c * width + (h + 1) * wide],
+            output_w.at[h, c * wide : (c + 1) * wide], load_sem.at[base + 1 + h * n_col + c])
+        for h in range(parts) for c in range(n_col)
     ]
-    for load in loads:
-        load.start()
-
+    for copy in small[:5] + [feature_load, first_load, last_load, token_load]:
+        copy.start()
+    for pair in weight_loads:
+        for copy in pair:
+            copy.start()
+    for copy in small[5:]:
+        copy.start()
+
+    for copy in small[:5]:
+        copy.wait()
     turn = frequency[...] * (0.5 / math.pi)
     high, low = split_two(feature_weight[...] * turn)
     phase_high, phase_low = split_two(feature_phase[...] * turn)
@@ -382,203 +415,294 @@
         inner_w.append(jnp.concatenate([
             jnp.concatenate([mat_high, mat_low], 1), jnp.concatenate([mat_high, jnp.zeros_like(mat_low)], 1)], 0))
     inner_p = inner_phase[...] * turn
-    chan[0] = forward[...].T
-    chan[1] = backward[...].T
-    rate_col[...] = jnp.broadcast_to(rate[...], (128, width)).T
-    own = pl.ds(pl.multiple_of(row * count, 16), count)
-    both_w = jnp.concatenate([chan[0, own, :], chan[1, own, :]], 0).astype(bf16)
-    rates = rate_col[own, 0:1]
-    chunk = 512
-    energy_ref[...] = jnp.zeros_like(energy_ref)
 
     def hidden_chunk(i):
-        at = pl.ds(i * chunk, chunk)
+        at = pl.ds(i * CHUNK, CHUNK)
         hidden = sine_of_turns(dot(feats[at, :], first_w))
         for level in range(INNER):
             h_high, h_low = split_two(hidden)
-            wide = dot(jnp.concatenate([h_high, h_low], 1), inner_w[level])
-            hidden = sine_of_turns(wide[:, :128] + wide[:, 128:] + inner_p[level : level + 1, :])
-        hid[col, at, :] = hidden.astype(bf16)
+            both = dot(jnp.concatenate([h_high, h_low], 1), inner_w[level])
+            hidden = sine_of_turns(both[:, :LANES] + both[:, LANES:] + inner_p[level : level + 1, :])
+        hid[side, at, :] = hidden.astype(bf16)
+
+    pieces = half // CHUNK
+    to_partner = []
+    for i in range(pieces):
+        part = hid.at[side, pl.ds(i * CHUNK, CHUNK)]
+        to_partner.append(pltpu.make_async_remote_copy(
+            src_ref=part, dst_ref=part, send_sem=hid_s.at[i], recv_sem=hid_r.at[i],
+            device_id=(row, partner), device_id_type=mesh_id))
+
+    feature_load.wait()
+    for i in range(pieces // 2):
+        hidden_chunk(i)
+    pl.semaphore_wait(barrier, n_row + n_col - 2)
+    first_load.wait()
+    last_load.wait()
+    ends = [tok[rows - 16 : rows].astype(f32)[15:16], tok[0:16].astype(f32)[0:1]]
+    for j, end in enumerate(ends):
+        for i in range(depth // LANES):
+            edge_ref[j, i : i + 1, :] = end[:, i * LANES : (i + 1) * LANES]
+        edge_out[j] = edge_ref[j].astype(bf16)
+    down = pltpu.make_async_remote_copy(
+        src_ref=edge_out.at[0], dst_ref=edge_in.at[0],
+        send_sem=edge_send.at[0], recv_sem=edge_recv.at[0],
+        device_id=(lax.rem(row + 1, n_row), col), device_id_type=mesh_id)
+    up = pltpu.make_async_remote_copy(
+        src_ref=edge_out.at[1], dst_ref=edge_in.at[1],
+        send_sem=edge_send.at[1], recv_sem=edge_recv.at[1],
+        device_id=(lax.rem(row + n_row - 1, n_row), col), device_id_type=mesh_id)
+
+    @pl.when(row < n_row - 1)
+    def _():
+        down.start()
+
+    @pl.when(row > 0)
+    def _():
+        up.start()
+
+    for i in range(pieces // 2):
+        to_partner[i].start()
+
+    token_load.wait()
+    for pair in weight_loads:
+        for copy in pair:
+            copy.wait()
+    for copy in [outer_load] + output_loads:
+        copy.start()
+    for h in range(parts):
+        proj_ref[h] = dot(tok[...], weights[h]).astype(bf16)
+
+    for copy in small[5:]:
+        copy.wait()
+    chan[0] = forward[...].T
+    chan[1] = backward[...].T
+    rate_col[...] = jnp.broadcast_to(rate[...], (LANES, width)).T
+    mine = [pl.ds(pl.multiple_of(h * wide + row * GROUP, GROUP), GROUP) for h in range(parts)]
+    both_w = jnp.concatenate([chan[j, own, :] for j in range(2) for own in mine], 0).astype(bf16)
+    rates = jnp.concatenate([rate_col[own, 0:1] for own in mine], 0)
+    energy_ref[...] = jnp.zeros_like(energy_ref)
+
+    @pl.when(row > 0)
+    def _():
+        down.wait_recv()
+
+    @pl.when(row < n_row - 1)
+    def _():
+        up.wait_recv()
+
+    for j in range(2):
+        edge_ref[j] = edge_in[j].astype(f32)
+        for i in range(depth // LANES):
+            end_ref[j : j + 1, i * LANES : (i + 1) * LANES] = edge_ref[j, i : i + 1, :]
+    end_rows = end_ref[...].astype(bf16)
+
+    index = lax.broadcasted_iota(jnp.int32, (rows, 2 * wide), 0)
+
+    def convolved(main, ends, tap):
+        first = jnp.where(row > 0, ends[0:1], 0.0)
+        last = jnp.where(row < n_row - 1, ends[1:2], 0.0)
+        at_row = index[:, : main.shape[1]]
+        before = jnp.where(at_row == 0, first, pltpu.roll(main, 1, 0))
+        after = jnp.where(at_row == rows - 1, last, pltpu.roll(main, rows - 1, 0))
+        return before * tap[0] + main * tap[1] + after * tap[2]
+
+    def rounded(value):
+        return value.astype(bf16).astype(f32)
+
+    other = 1 - lax.div(row, n_row // 2)
+    place = lax.rem(row, n_row // 2)
+    peers = [other * (n_row // 2) + lax.rem(place + i, n_row // 2) for i in range(n_row // 2)]
+    peers += [(1 - other) * (n_row // 2) + lax.rem(place + i, n_row // 2) for i in range(1, n_row // 2)]
+
+    sig_copies = []
+    for h in range(parts):
+        ends = rounded(dot(end_rows, weights[h]))
+        at = slice(h * wide, (h + 1) * wide)
+        tap = [jnp.concatenate([taps[i, 1:2, at], taps[i, 2:3, at]], 1) for i in range(3)]
+        made = convolved(proj_ref[h].astype(f32), ends, tap)
+        signal = (made[:, :wide] * made[:, wide:]).astype(bf16).astype(f32).T
+        signal_ref[h] = signal
+        flipped = signal.astype(bf16)
+        for g in range(n_row):
+            sig_send[h, g] = flipped[g * GROUP : (g + 1) * GROUP]
+        for i, peer in enumerate(peers):
+            sig_copies.append(pltpu.make_async_remote_copy(
+                src_ref=sig_send.at[h, peer], dst_ref=sig_recv.at[h, row],
+                send_sem=sig_s.at[h, i], recv_sem=sig_r.at[h, i],
+                device_id=(peer, col), device_id_type=mesh_id))
+            sig_copies[-1].start()
+        sig_recv[h, row] = sig_send[h, row]
+
+    outer_load.wait()
+    skip_col = jnp.broadcast_to(skip[...], (LANES, width)).T
+    for h in range(parts):
+        at = slice(h * wide, (h + 1) * wide)
+        main = rounded(dot(tok[...], outer_w[:, at]))
+        ends = rounded(dot(end_rows, outer_w[:, at]))
+        gate = rounded(convolved(main, ends, [taps[i, 0:1, at] for i in range(3)])).T.astype(bf16)
+        direct = (signal_ref[h] * skip_col[at, 0:1]).astype(bf16)
+        for p in range(n_col):
+            gs_send[p, 0, h] = gate[:, p * share : (p + 1) * share]
+            gs_send[p, 1, h] = direct[:, p * share : (p + 1) * share]
+    gs_copies = []
+    for o in range(1, n_col):
+        peer = lax.rem(col + o, n_col)
+        gs_copies.append(pltpu.make_async_remote_copy(
+            src_ref=gs_send.at[peer], dst_ref=gs_recv.at[col],
+            send_sem=gs_s.at[o], recv_sem=gs_r.at[o], device_id=(row, peer), device_id_type=mesh_id))
+        gs_copies[-1].start()
+    gs_recv[col] = gs_send[col]
+
+    for i in range(pieces // 2, pieces):
+        hidden_chunk(i)
+        to_partner[i].start()
 
     def filter_chunk(owner, i):
-        at = pl.ds(pl.multiple_of(owner * quarter + i * chunk, chunk), chunk)
-        both = lax.dot_general(both_w, hid[owner, pl.ds(i * chunk, chunk), :], (((1,), (1,)), ((), ())),
+        start = owner * half + i * CHUNK
+        at = pl.ds(pl.multiple_of(start, CHUNK), CHUNK)
+        both = lax.dot_general(both_w, hid[owner, pl.ds(i * CHUNK, CHUNK), :], (((1,), (1,)), ((), ())),
                                preferred_element_type=f32)
-        place = lax.broadcasted_iota(jnp.int32, (count, chunk), 1) + (owner * quarter + i * chunk)
+        place = lax.broadcasted_iota(jnp.int32, (count, CHUNK), 1) + start
         window = jnp.exp(place.astype(f32) * (-1.0 / (length - 1)) * rates)
         ahead = both[:count] * window
         behind = jnp.where(place == 0, 0.0, both[count:] * window)
         sums[:, at] = ahead + behind
         diffs[:, at] = ahead - behind
         energy_ref[...] += jnp.broadcast_to(
-            jnp.sum(ahead * ahead + behind * behind, axis=1, keepdims=True), (count, 128))
-
-    pieces = quarter // chunk
-    partner = col + 1 - 2 * lax.rem(col, 2)
-    across = lax.rem(col + 2, n_col)
-
-    def pass_on(kind, owner, i, target):
-        part = hid.at[owner, pl.ds(i * chunk, chunk)]
-        return pltpu.make_async_remote_copy(
-            src_ref=part, dst_ref=part, send_sem=hid_s.at[kind, i], recv_sem=hid_r.at[kind, i],
-            device_id=(row, target), device_id_type=mesh_id)
-
-    loads[0].wait()
+            jnp.sum(ahead * ahead + behind * behind, axis=1, keepdims=True), (count, LANES))
+
     for i in range(pieces):
-        hidden_chunk(i)
-
-    pl.semaphore_wait(barrier, n_row + n_col - 2)
-    edges = [
-        pltpu.make_async_remote_copy(
-            src_ref=tokens_h.at[pl.ds(rows - 16 if i == 0 else 0, 16)],
-            dst_ref=tok.at[pl.ds(rows + 16 * i, 16)],
-            send_sem=edge_send.at[i], recv_sem=edge_recv.at[i],
-            device_id=(lax.rem(row + (1 if i == 0 else n_row - 1), n_row), col), device_id_type=mesh_id)
-        for i in range(2)
-    ]
-    for edge in edges:
-        edge.start()
-    to_across = [pass_on(0, col, i, across) for i in range(pieces)]
-    to_partner = [pass_on(1, col, i, partner) for i in range(pieces)]
-    relayed = [pass_on(2, across, i, partner) for i in range(pieces)]
-    for copy in to_across + to_partner:
-        copy.start()
-    loads[1].wait()
-    loads[2].wait()
-    loads[3].wait()
-    for edge in edges:
-        edge.wait()
-
-    index = lax.broadcasted_iota(jnp.int32, (rows, width), 0)
-    has_before = jnp.where(row > 0, 1.0, 0.0)
-    has_after = jnp.where(row < n_row - 1, 1.0, 0.0)
-
-    def convolved(j):
-        proj = dot(tok[...], weights[j]).astype(bf16).astype(f32)
-        main = proj[:rows]
-        first = proj[rows + 15 : rows + 16] * has_before
-        last = proj[rows + 16 : rows + 17] * has_after
-        before = jnp.where(index == 0, first, pltpu.roll(main, 1, 0))
-        after = jnp.where(index == rows - 1, last, pltpu.roll(main, rows - 1, 0))
-        return before * taps[0, j : j + 1, :] + main * taps[1, j : j + 1, :] + after * taps[2, j : j + 1, :]
-
-    signal = (convolved(1) * convolved(2)).astype(bf16)
-    signal_ref[...] = signal
-    flipped = signal.astype(f32).T.astype(bf16)
-    for g in range(n_row):
-        sig_send[g] = flipped[g * count : (g + 1) * count]
-
-    def exchange(send, recv, s_sem, r_sem, size, me, target):
-        copies = []
-        for o in range(1, size):
-            peer = lax.rem(me + o, size)
-            copies.append(pltpu.make_async_remote_copy(
-                src_ref=send.at[peer], dst_ref=recv.at[me],
-                send_sem=s_sem.at[o], recv_sem=r_sem.at[o], device_id=target(peer), device_id_type=mesh_id))
-        for copy in copies:
-            copy.start()
-        recv[me] = send[me]
-        return copies
-
-    along_row = lambda peer: (peer, col)
-    along_col = lambda peer: (row, peer)
-    travelling = exchange(sig_send, sig_recv, sig_s, sig_r, n_row, row, along_row)
-
-    loads[4].wait()
-    gate_ref[...] = convolved(0).astype(bf16)
+        filter_chunk(side, i)
     for i in range(pieces):
-        filter_chunk(col, i)
-    for i in range(pieces):
-        to_partner[i].wait()
-        filter_chunk(partner, i)
-    for i in range(pieces):
-        to_across[i].wait()
-        relayed[i].start()
-    for i in range(pieces):
-        filter_chunk(across, i)
-    for i in range(pieces):
-        relayed[i].wait()
-        filter_chunk(lax.rem(partner + 2, n_col), i)
+        to_partner[i].wait_recv()
+        filter_chunk(1 - side, i)
     scale_ref[...] = lax.rsqrt(1.0 + energy_ref[...]) * (0.5 / length)
 
-    def turn_into(first, pairs, top, left, weighted):
+    def turn_into(first, pairs, base_row, left, weighted):
         for k, (real, imag) in enumerate(pairs):
-            c, s = twist_c[k : k + 1, pl.ds(left, 128)], twist_s[k : k + 1, pl.ds(left, 128)]
+            c, s = twist[0, k : k + 1, pl.ds(left, LANES)], twist[1, k : k + 1, pl.ds(left, LANES)]
             if weighted and k not in (0, planes):
                 c, s = c * 2.0, s * 2.0
-            at = pl.ds(pl.multiple_of(k * count + top, 16), 16)
+            at = pl.ds(pl.multiple_of(base_row + k * GROUP, GROUP), GROUP)
             if imag is None:
                 new_real, new_imag = real * c, -(real * s)
             else:
                 new_real, new_imag = real * c + imag * s, imag * c - real * s
-            turned[first, at, pl.ds(left, 128)] = new_real.astype(bf16)
-            turned[first + 1, at, pl.ds(left, 128)] = new_imag.astype(bf16)
-
-    def filter_tile(top, left):
-        scale = scale_ref[pl.ds(top, 16), :]
+            turned[first, at, pl.ds(left, LANES)] = new_real.astype(bf16)
+            turned[first, at, pl.ds(pl.multiple_of(WIDE + left, LANES), LANES)] = new_imag.astype(bf16)
+
+    lanes = WIDE // LANES
+
+    def filter_tile(i, carry):
+        h, left = i // lanes, pl.multiple_of(i % lanes * LANES, LANES)
+        top = pl.ds(pl.multiple_of(h * GROUP, GROUP), GROUP)
+        scale = scale_ref[top, :]
         for which, source in enumerate((sums, diffs)):
-            got = [source[pl.ds(top, 16), pl.ds(pl.multiple_of(r * WIDE + left, 128), 128)] * scale for r in range(planes)]
-            turn_into(2 * which, first_stage(got), top, left, True)
-
-    tiles(count, filter_tile)
-    filt[0] = dot(turned[0], cos_t[...]) + dot(turned[1], sin_t[...])
-    filt[1] = dot(turned[3], cos_t[...]) - dot(turned[2], sin_t[...])
-    for copy in travelling:
+            got = [source[top, pl.ds(pl.multiple_of(r * WIDE + left, LANES), LANES)] * scale for r in range(planes)]
+            turn_into(which, first_stage(got), h * spec, left, True)
+        return carry
+
+    lax.fori_loop(0, parts * lanes, filter_tile, 0)
+    filt[0] = dot(turned[0], trig[:, :WIDE])
+    filt[1] = dot(turned[1], trig[:, WIDE:])
+
+    resp_copies = []
+    for h in range(parts):
+        for copy in sig_copies[h * (n_row - 1) : (h + 1) * (n_row - 1)]:
+            copy.wait_recv()
+        band = pl.ds(h * spec, spec)
+
+        def signal_tile(i, carry):
+            left = pl.multiple_of(i * LANES, LANES)
+            got = [sig_recv[h, r // per, :, pl.ds(pl.multiple_of(r % per * WIDE + left, LANES), LANES)].astype(f32)
+                   for r in range(planes)]
+            turn_into(0, first_stage(got), h * spec, left, False)
+            return carry
+
+        lax.fori_loop(0, lanes, signal_tile, 0)
+        spectrum = dot(turned[0, band], trig[...])
+        real, imag = spectrum[:, :WIDE], spectrum[:, WIDE:]
+        prod_real = (real * filt[0, band] - imag * filt[1, band]).astype(bf16)
+        prod_imag = (real * filt[1, band] + imag * filt[0, band]).astype(bf16)
+        back[...] = dot(jnp.concatenate([prod_imag, prod_real], 1), trig[...])
+
+        def back_tile(i, carry):
+            left = pl.multiple_of(i * LANES, LANES)
+            pairs = []
+            for k in range(planes + 1):
+                c, s = twist[0, k : k + 1, pl.ds(left, LANES)], twist[1, k : k + 1, pl.ds(left, LANES)]
+                at = pl.ds(k * GROUP, GROUP)
+                b_imag, b_real = back[at, pl.ds(left, LANES)], back[at, pl.ds(pl.multiple_of(WIDE + left, LANES), LANES)]
+                pairs.append((b_real * c - b_imag * s, b_imag * c + b_real * s))
+            for r, plane in enumerate(last_stage(pairs)):
+                resp_send[h, r // per, r % per * lanes + i] = plane.astype(bf16)
+            return carry
+
+        lax.fori_loop(0, lanes, back_tile, 0)
+        for i, peer in enumerate(peers + [row]):
+            for o in range(n_col):
+                if i == n_row - 1 and o == 0:
+                    continue
+                target = lax.rem(col + o, n_col)
+                resp_copies.append(pltpu.make_async_remote_copy(
+                    src_ref=resp_send.at[h, peer, target], dst_ref=resp_recv.at[h, col, row],
+                    send_sem=resp_s.at[h], recv_sem=resp_r.at[h, col],
+                    device_id=(peer, target), device_id_type=mesh_id))
+                resp_copies[-1].start()
+        resp_recv[h, col, row] = resp_send[h, row, col]
+
+    for copy in gs_copies:
+        copy.wait_recv()
+    for copy in output_loads:
         copy.wait()
-
-    def signal_tile(top, left):
-        got = [sig_recv[r // per, pl.ds(top, 16), pl.ds(pl.multiple_of(r % per * WIDE + left, 128), 128)].astype(f32)
-               for r in range(planes)]
-        turn_into(0, first_stage(got), top, left, False)
-
-    tiles(count, signal_tile)
-    real = dot(turned[0], cos_t[...]) + dot(turned[1], sin_t[...])
-    imag = dot(turned[1], cos_t[...]) - dot(turned[0], sin_t[...])
-    prod_real = (real * filt[0] - imag * filt[1]).astype(bf16)
-    prod_imag = (real * filt[1] + imag * filt[0]).astype(bf16)
-    back[0] = dot(prod_real, cos_t[...]) - dot(prod_imag, sin_t[...])
-    back[1] = dot(prod_imag, cos_t[...]) + dot(prod_real, sin_t[...])
-
-    def back_tile(top, left):
-        pairs = []
-        for k in range(planes + 1):
-            c, s = twist_c[k : k + 1, pl.ds(left, 128)], twist_s[k : k + 1, pl.ds(left, 128)]
-            at = pl.ds(pl.multiple_of(k * count + top, 16), 16)
-            b_real, b_imag = back[0, at, pl.ds(left, 128)], back[1, at, pl.ds(left, 128)]
-            pairs.append((b_real * c - b_imag * s, b_imag * c + b_real * s))
-        for r, plane in enumerate(last_stage(pairs)):
-            at = pl.multiple_of(r % per * WIDE + left, 128)
-            resp_send[r // per, pl.ds(top, 16), pl.ds(at, 128)] = plane.astype(bf16)
-
-    tiles(count, back_tile)
-    for copy in exchange(resp_send, resp_recv, resp_s, resp_r, n_row, row, along_row):
-        copy.wait()
-    response = jnp.concatenate([resp_recv[g].astype(f32) for g in range(n_row)], 0).T
-    mixed = (gate_ref[...].astype(f32) * (response + skip[...] * signal_ref[...].astype(f32))).astype(bf16)
-    share = rows // n_col
-    for p in range(n_col):
-        mix_send[p] = mixed[p * share : (p + 1) * share]
-    travelling = exchange(mix_send, mix_recv, mix_s, mix_r, n_col, col, along_col)
-    for copy in travelling:
-        copy.wait()
-    for p in range(n_col):
-        out_ref[:, p * width : (p + 1) * width] = mix_recv[p]
+    for h in range(parts):
+        for o in range(n_col):
+            source = lax.rem(col + o, n_col)
+            come = resp_recv.at[h, source, pl.ds(0, n_row - 1 if o == 0 else n_row)]
+            pltpu.make_async_copy(come, come, resp_r.at[h, source]).wait()
+        shape = (n_col * wide, share)
+        response = resp_recv[h].reshape(shape).astype(f32)
+        gate, direct = (gs_recv[:, j, h].reshape(shape).astype(f32) for j in range(2))
+        mixed = (gate * (response + direct)).T.astype(bf16)
+        got = dot(mixed, output_w[h])
+        if h == 0:
+            total_ref[...] = got
+        elif h < parts - 1:
+            total_ref[...] += got
+        else:
+            out_ref[...] = (total_ref[...] + got).astype(bf16)
+
+    @pl.when(row < n_row - 1)
+    def _():
+        down.wait_send()
+
+    @pl.when(row > 0)
+    def _():
+        up.wait_send()
+
+    for copy in to_partner + sig_copies + gs_copies:
+        copy.wait_send()
+    for h in range(parts):
+        gone = resp_send.at[h].reshape(n_row * n_col, GROUP, share).at[pl.ds(0, n_row * n_col - 1)]
+        pltpu.make_async_copy(gone, gone, resp_s.at[h]).wait()
 
 
 def fits(tokens_rows, seq_length, own_width, row_devices, col_devices, units):
     planes = seq_length // WIDE
     members = own_width // row_devices
     return (
-        own_width % 128 == 0
-        and members % 16 == 0
+        members % (2 * GROUP) == 0
+        and own_width % row_devices == 0
+        and row_devices * GROUP % LANES == 0
+        and row_devices % 2 == 0
         and tokens_rows % WIDE == 0
-        and seq_length % 512 == 0
         and planes % 8 == 0
         and 8 <= planes <= 32
-        and units == 128
-        and tokens_rows % 64 == 0
+        and units == LANES
         and col_devices == 4
-        and seq_length % 2048 == 0
+        and tokens_rows == col_devices * LANES
+        and seq_length % (4 * CHUNK) == 0
     )
 
 
@@ -592,60 +716,71 @@
     seq_length = rows * devices
     width = outer_weight.shape[1]
     members = width // devices
+    parts = members // GROUP
+    wide = width // parts
     planes = seq_length // WIDE
     n_col = lax.axis_size("col")
     k_index = np.arange(planes + 1)[:, None] * np.arange(WIDE)[None, :]
-    twist_c = jnp.asarray(np.cos(2 * np.pi * k_index / (2 * seq_length)), f32)
-    twist_s = jnp.asarray(np.sin(2 * np.pi * k_index / (2 * seq_length)), f32)
-    w_index = np.arange(WIDE)[:, None] * np.arange(WIDE)[None, :] % WIDE
-    cos_t = jnp.asarray(np.cos(2 * np.pi * w_index / WIDE), bf16)
-    sin_t = jnp.asarray(np.sin(2 * np.pi * w_index / WIDE), bf16)
-    spec_rows = (planes + 1) * members
+    twist_angle = 2 * np.pi * k_index / (2 * seq_length)
+    twist = jnp.asarray(np.stack([np.cos(twist_angle), np.sin(twist_angle)]), f32)
+    w_angle = 2 * np.pi * (np.arange(WIDE)[:, None] * np.arange(WIDE)[None, :] % WIDE) / WIDE
+    cos_w, sin_w = np.cos(w_angle), np.sin(w_angle)
+    trig = jnp.asarray(np.block([[cos_w, -sin_w], [sin_w, cos_w]]), bf16)
+    spec = (planes + 1) * GROUP
     any_spec = pl.BlockSpec(memory_space=pl.ANY)
     vmem = pl.BlockSpec(memory_space=pltpu.VMEM)
     dma = pltpu.SemaphoreType.DMA
     share = rows // n_col
-    pieces = seq_length // n_col // 512
-    exchanged = pltpu.VMEM((devices, members, rows), bf16)
-    spread = pltpu.VMEM((n_col, share, width), bf16)
-    mixed = pl.pallas_call(
+    half = seq_length // 2
+    pieces = half // CHUNK
+    small = [
+        conv_taps, feature_weight, feature_phase[None], inner_mats, inner_phase, frequency[None],
+        forward_weight, backward_weight, decay_rate[None], skip_gain[None], twist, trig]
+    exchanged = pltpu.VMEM((parts, devices, GROUP, rows), bf16)
+    spread = pltpu.VMEM((n_col, 2, parts, wide, share), bf16)
+    return pl.pallas_call(
         layer_kernel,
-        out_shape=jax.ShapeDtypeStruct((share, n_col * width), bf16),
-        in_specs=[any_spec] * 5 + [vmem] * 14,
+        out_shape=pltpu.VMEM((share, output_weight.shape[1]), bf16),
+        in_specs=[any_spec] * (6 + len(small)),
         out_specs=vmem,
         scratch_shapes=[
-            pltpu.VMEM((rows + 32, depth), bf16),
-            pltpu.VMEM((3, depth, width), bf16),
-            pltpu.VMEM((seq_length // n_col, 128), bf16),
-            pltpu.VMEM((n_col, seq_length // n_col, 128), bf16),
-            exchanged, exchanged, exchanged, exchanged, spread, spread,
+            pltpu.VMEM((rows, depth), bf16),
+            pltpu.VMEM((parts, depth, 2 * wide), bf16),
+            pltpu.VMEM((depth, width), bf16),
+            pltpu.VMEM((half, LANES), bf16),
+            pltpu.VMEM((parts, n_col * wide, output_weight.shape[1]), bf16),
+        ] + [pltpu.VMEM(a.shape, a.dtype) for a in small] + [
+            pltpu.VMEM((2, half, LANES), bf16),
+            exchanged, exchanged, spread, spread,
+            pltpu.VMEM((parts, devices, n_col, GROUP, share), bf16),
+            pltpu.VMEM((parts, n_col, devices, GROUP, share), bf16),
             pltpu.VMEM((members, seq_length), f32),
             pltpu.VMEM((members, seq_length), f32),
-            pltpu.VMEM((4, spec_rows, WIDE), bf16),
-            pltpu.VMEM((2, spec_rows, WIDE), f32),
-            pltpu.VMEM((2, spec_rows, WIDE), f32),
-            pltpu.VMEM((members, 128), f32),
-            pltpu.VMEM((128, 128), f32),
-            pltpu.VMEM((2, width, 128), f32),
-            pltpu.VMEM((width, 128), f32),
-            pltpu.VMEM((members, 128), f32),
-            pltpu.VMEM((rows, width), bf16),
-            pltpu.VMEM((rows, width), bf16),
-            dma((5,)), dma((2,)), dma((2,)), dma((3, pieces)), dma((3, pieces)),
-            dma((devices,)), dma((devices,)), dma((devices,)), dma((devices,)), dma((n_col,)), dma((n_col,)),
+            pltpu.VMEM((2, parts * spec, 2 * WIDE), bf16),
+            pltpu.VMEM((2, parts * spec, WIDE), f32),
+            pltpu.VMEM((spec, 2 * WIDE), f32),
+            pltpu.VMEM((members, LANES), f32),
+            pltpu.VMEM((LANES, LANES), f32),
+            pltpu.VMEM((2, width, LANES), f32),
+            pltpu.VMEM((width, LANES), f32),
+            pltpu.VMEM((members, LANES), f32),
+            pltpu.VMEM((parts, rows, 2 * wide), bf16),
+            pltpu.VMEM((parts, wide, rows), f32),
+            pltpu.VMEM((share, output_weight.shape[1]), f32),
+            pltpu.VMEM((2, depth // LANES, LANES), f32),
+            pltpu.VMEM((2, depth // LANES, LANES), bf16),
+            pltpu.VMEM((2, depth // LANES, LANES), bf16),
+            pltpu.VMEM((16, depth), f32),
+            dma((5 + 2 * parts + parts * n_col,)), dma((len(small),)), dma((2,)), dma((2,)), dma((pieces,)), dma((pieces,)),
+            dma((parts, devices)), dma((parts, devices)), dma((n_col,)), dma((n_col,)), dma((parts,)), dma((parts, n_col)),
         ],
         compiler_params=pltpu.CompilerParams(
             collective_id=0, has_side_effects=True, vmem_limit_bytes=GRANT),
         name="layer",
-    )(
-        tokens, outer_weight, inner_weight, value_weight, jnp.asarray(feature_table(seq_length)),
-        conv_taps, feature_weight, feature_phase[None], inner_mats, inner_phase, frequency[None],
-        forward_weight, backward_weight, decay_rate[None], skip_gain[None], twist_c, twist_s, cos_t, sin_t,
-    )
-    return jnp.dot(mixed, output_weight, preferred_element_type=f32).astype(bf16)
-
-
-GRANT = 54 * 1024 * 1024
+    )(tokens, outer_weight, inner_weight, value_weight, jnp.asarray(feature_table(seq_length)), output_weight, *small)
+
+
+GRANT = 58 * 1024 * 1024
 
 
 def on_any(*args):

time: 36.6 us -> 28.3 us (0.77)
  Pallas kernels: 33.9 us -> 27.4 us
  matrix products: 2.47 us -> 0 us
  local copies, waits for them, and re-layouts: 0.01 us -> 0.8 us
    pallas_call x1, Pallas kernels: 33.9 us -> 27.4 us  [on_device_fast(): pl.pallas_call(layer_kernel, out_shape=pltpu.VMEM((share, output_weight.s...]
    dot_general x1 -> x0, matrix products: 2.47 us -> none  [on_device_fast(): jnp.dot(mixed, output_weight, preferred_element_type=f32).astype(bf16)]
    unnamed x2 -> x1, local copies, waits for them, and re-layouts: 0.01 us -> 0.8 us
where the time goes in v1:
time: 28.3 us; the launch traced here: 28.2 us
  Pallas kernels  27.4 us (97%)
  local copies, waits for them, and re-layouts  0.8 us (3%)
    pallas_call x1, Pallas kernels, on_device_fast(): pl.pallas_call(layer_kernel, out_shape=pltpu.VMEM((share, output_weight.s...  27.4 us
    unnamed x1, local copies, waits for them, and re-layouts  0.8 us

profile of v1, /device:TPU:0, one launch (start us, length us, event | category | flops | bytes accessed | tf_op | source)
XLA Modules:
  0.0 28.2 jit_solution(7811863557212733364)
XLA Ops:
  0.0 27.4 %layer.1 = bf16[128,2048]{1,0:T(8,128)(2,1)S(1)} custom-call(bf16[512,2048]{1,0:T(8,128)(2,1)} %tokens_h.1, bf16[2048,256]{1,0:T(8,128)(2,1)} %outer_h.1, bf16[2048,256]{1,0:T(8,128)(2,1)} %inner_h.1, bf16[2048,256]{1,0:T(8,128)(2,1)} %value_h.1, bf16[4096,128]{1,0:T(8,128)(2,1)} %constant.8.clone.feats_h, bf16[1024,2048]{1,0:T(8,128)(2,1)} %output_h.1, ...), custom_call_target="tpu_custom_call" | custom-call | tf_op jit(solution)/shard_map/layer/pallas_call | solution.py:741
  27.4 0.8 %copy.20 = bf16[128,2048]{1,0:T(8,128)(2,1)} copy(bf16[128,2048]{1,0:T(8,128)(2,1)S(1)} %layer.1) | data formatting | bytes 1048576

commit v2 on v1

--- a/solution.py
+++ b/solution.py
@@ -319,6 +319,8 @@
 
 
 GROUP = 16
+REACH = 2
+ROUNDS = 2
 LANES = 128
 CHUNK = 512
 
@@ -331,9 +333,9 @@
     tok, weights, outer_w, feats, output_w, taps, feature_weight, feature_phase, inner_mats, inner_phase, frequency,
     forward, backward, rate, skip, twist, trig,
     hid, sig_send, sig_recv, gs_send, gs_recv, resp_send, resp_recv,
-    sums, diffs, turned, filt, back, scale_ref, first_ref, chan, rate_col, energy_ref, proj_ref, signal_ref, total_ref,
+    sums, diffs, turned, filt, back, scale_ref, first_ref, chan, rate_col, energy_ref, signal_ref, total_ref,
     edge_ref, edge_out, edge_in, end_ref,
-    load_sem, small_sem, edge_send, edge_recv, hid_s, hid_r, sig_s, sig_r, gs_s, gs_r, resp_s, resp_r,
+    load_sem, small_sem, edge_send, edge_recv, hid_s, hid_r, sig_s, sig_r, gs_s, gs_r, resp_s, resp_r, alive,
 ):
     f32, bf16 = jnp.float32, jnp.bfloat16
     dot = functools.partial(jnp.dot, preferred_element_type=f32)
@@ -349,12 +351,31 @@
     planes = length // WIDE
     per = rows // WIDE
     share = rows // n_col
+    halves = width // LANES
+    pair = parts // halves
     spec = (planes + 1) * GROUP
     mesh_id = pl.DeviceIdType.MESH
 
+    def arrived(ref, semaphore):
+        pltpu.make_async_copy(ref, ref, semaphore).wait()
+
     barrier = pltpu.get_barrier_semaphore()
-    for o in range(1, n_row):
-        pl.semaphore_signal(barrier, inc=1, device_id=(lax.rem(row + o, n_row), col), device_id_type=mesh_id)
+    reach = REACH
+
+    def along(step, semaphore):
+        @pl.when(row >= step)
+        def _():
+            pl.semaphore_signal(semaphore, inc=1, device_id=(row - step, col), device_id_type=mesh_id)
+
+        @pl.when(row < n_row - step)
+        def _():
+            pl.semaphore_signal(semaphore, inc=1, device_id=(row + step, col), device_id_type=mesh_id)
+
+    def either(step):
+        return jnp.where(row >= step, 1, 0) + jnp.where(row < n_row - step, 1, 0)
+
+    for step in range(1, reach + 1):
+        along(step, barrier)
     for o in range(1, n_col):
         pl.semaphore_signal(barrier, inc=1, device_id=(row, lax.rem(col + o, n_col)), device_id_type=mesh_id)
     side = lax.rem(col, 2)
@@ -369,32 +390,59 @@
     feature_load = pltpu.make_async_copy(
         feats_h.at[pl.ds(pl.multiple_of(side * half, CHUNK), half)], feats, load_sem.at[0])
     first_load = pltpu.make_async_copy(tokens_h.at[0:16], tok.at[0:16], load_sem.at[1])
-    last_load = pltpu.make_async_copy(tokens_h.at[rows - 16 : rows], tok.at[rows - 16 : rows], load_sem.at[2])
-    token_load = pltpu.make_async_copy(tokens_h.at[16 : rows - 16], tok.at[16 : rows - 16], load_sem.at[3])
+    last_load = pltpu.make_async_copy(tokens_h.at[rows - 16 : rows], tok.at[rows - 16 : rows], load_sem.at[1])
+    token_load = pltpu.make_async_copy(tokens_h.at[16 : rows - 16], tok.at[16 : rows - 16], load_sem.at[2])
     weight_loads = [
         [
             pltpu.make_async_copy(
-                source.at[:, h * wide : (h + 1) * wide], weights.at[h, :, j * wide : (j + 1) * wide],
-                load_sem.at[4 + 2 * h + j])
+                source.at[:, h * LANES : (h + 1) * LANES], weights.at[h, :, j * LANES : (j + 1) * LANES],
+                load_sem.at[3 + h])
             for j, source in enumerate((inner_h, value_h))
         ]
-        for h in range(parts)
+        for h in range(halves)
     ]
-    base = 4 + 2 * parts
+    base = 3 + halves
     outer_load = pltpu.make_async_copy(outer_h, outer_w, load_sem.at[base])
     output_loads = [
         pltpu.make_async_copy(
             output_h.at[c * width + h * wide : c * width + (h + 1) * wide],
-            output_w.at[h, c * wide : (c + 1) * wide], load_sem.at[base + 1 + h * n_col + c])
+            output_w.at[h, c * wide : (c + 1) * wide], load_sem.at[base + 1])
         for h in range(parts) for c in range(n_col)
     ]
-    for copy in small[:5] + [feature_load, first_load, last_load, token_load]:
+    for copy in [first_load, last_load] + small[:5] + [feature_load, token_load]:
         copy.start()
-    for pair in weight_loads:
-        for copy in pair:
-            copy.start()
+    for copy in sum(weight_loads, []):
+        copy.start()
     for copy in small[5:]:
         copy.start()
+
+    arrived(tok.at[0:32], load_sem.at[1])
+    ends = [tok[rows - 16 : rows].astype(f32)[15:16], tok[0:16].astype(f32)[0:1]]
+    for j, end in enumerate(ends):
+        for i in range(depth // LANES):
+            edge_ref[j, i : i + 1, :] = end[:, i * LANES : (i + 1) * LANES]
+        edge_out[j] = edge_ref[j].astype(bf16)
+    pl.semaphore_wait(barrier, n_col - 1 + either(1) + either(2))
+    down = pltpu.make_async_remote_copy(
+        src_ref=edge_out.at[0], dst_ref=edge_in.at[0],
+        send_sem=edge_send.at[0], recv_sem=edge_recv.at[0],
+        device_id=(lax.rem(row + 1, n_row), col), device_id_type=mesh_id)
+    up = pltpu.make_async_remote_copy(
+        src_ref=edge_out.at[1], dst_ref=edge_in.at[1],
+        send_sem=edge_send.at[1], recv_sem=edge_recv.at[1],
+        device_id=(lax.rem(row + n_row - 1, n_row), col), device_id_type=mesh_id)
+
+    @pl.when(row < n_row - 1)
+    def _():
+        down.start()
+
+    @pl.when(row > 0)
+    def _():
+        up.start()
+
+    along(reach, alive.at[0])
+    known = 2 * reach
+    rounds = 1
 
     for copy in small[:5]:
         copy.wait()
@@ -430,48 +478,45 @@
     for i in range(pieces):
         part = hid.at[side, pl.ds(i * CHUNK, CHUNK)]
         to_partner.append(pltpu.make_async_remote_copy(
-            src_ref=part, dst_ref=part, send_sem=hid_s.at[i], recv_sem=hid_r.at[i],
+            src_ref=part, dst_ref=part, send_sem=hid_s.at[0], recv_sem=hid_r.at[0],
             device_id=(row, partner), device_id_type=mesh_id))
 
     feature_load.wait()
-    for i in range(pieces // 2):
+    for i in range(pieces - 1):
         hidden_chunk(i)
-    pl.semaphore_wait(barrier, n_row + n_col - 2)
-    first_load.wait()
-    last_load.wait()
-    ends = [tok[rows - 16 : rows].astype(f32)[15:16], tok[0:16].astype(f32)[0:1]]
-    for j, end in enumerate(ends):
-        for i in range(depth // LANES):
-            edge_ref[j, i : i + 1, :] = end[:, i * LANES : (i + 1) * LANES]
-        edge_out[j] = edge_ref[j].astype(bf16)
-    down = pltpu.make_async_remote_copy(
-        src_ref=edge_out.at[0], dst_ref=edge_in.at[0],
-        send_sem=edge_send.at[0], recv_sem=edge_recv.at[0],
-        device_id=(lax.rem(row + 1, n_row), col), device_id_type=mesh_id)
-    up = pltpu.make_async_remote_copy(
-        src_ref=edge_out.at[1], dst_ref=edge_in.at[1],
-        send_sem=edge_send.at[1], recv_sem=edge_recv.at[1],
-        device_id=(lax.rem(row + n_row - 1, n_row), col), device_id_type=mesh_id)
-
-    @pl.when(row < n_row - 1)
-    def _():
-        down.start()
-
-    @pl.when(row > 0)
-    def _():
-        up.start()
-
-    for i in range(pieces // 2):
         to_partner[i].start()
-
+    while known < n_row - 1:
+        pl.semaphore_wait(alive.at[rounds - 1], either(known // 2))
+        along(known, alive.at[rounds])
+        known, rounds = 2 * known, rounds + 1
     token_load.wait()
-    for pair in weight_loads:
-        for copy in pair:
-            copy.wait()
+    arrived(weights.at[0], load_sem.at[3])
     for copy in [outer_load] + output_loads:
         copy.start()
-    for h in range(parts):
-        proj_ref[h] = dot(tok[...], weights[h]).astype(bf16)
+    index = lax.broadcasted_iota(jnp.int32, (rows, 2 * LANES), 0)
+
+    def halved(matrix):
+        return jnp.concatenate([dot(tok[: rows // 2], matrix), dot(tok[rows // 2 :], matrix)], 0)
+
+    def edged(matrix):
+        middle = depth // 2
+        return dot(end_rows[:, :middle], matrix[:middle]) + dot(end_rows[:, middle:], matrix[middle:])
+
+    def convolved(main, ends, tap):
+        first = jnp.where(row > 0, ends[0:1], 0.0)
+        last = jnp.where(row < n_row - 1, ends[1:2], 0.0)
+        at_row = index[:, : main.shape[1]]
+        before = jnp.where(at_row == 0, first, pltpu.roll(main, 1, 0))
+        after = jnp.where(at_row == rows - 1, last, pltpu.roll(main, rows - 1, 0))
+        return before * tap[0] + main * tap[1] + after * tap[2]
+
+    def rounded(value):
+        return value.astype(bf16).astype(f32)
+
+    other = 1 - lax.div(row, n_row // 2)
+    place = lax.rem(row, n_row // 2)
+    peers = [other * (n_row // 2) + lax.rem(place + i, n_row // 2) for i in range(n_row // 2)]
+    peers += [(1 - other) * (n_row // 2) + lax.rem(place + i, n_row // 2) for i in range(1, n_row // 2)]
 
     for copy in small[5:]:
         copy.wait()
@@ -483,80 +528,63 @@
     rates = jnp.concatenate([rate_col[own, 0:1] for own in mine], 0)
     energy_ref[...] = jnp.zeros_like(energy_ref)
 
-    @pl.when(row > 0)
-    def _():
-        down.wait_recv()
-
-    @pl.when(row < n_row - 1)
-    def _():
-        up.wait_recv()
-
-    for j in range(2):
-        edge_ref[j] = edge_in[j].astype(f32)
-        for i in range(depth // LANES):
-            end_ref[j : j + 1, i * LANES : (i + 1) * LANES] = edge_ref[j, i : i + 1, :]
-    end_rows = end_ref[...].astype(bf16)
-
-    index = lax.broadcasted_iota(jnp.int32, (rows, 2 * wide), 0)
-
-    def convolved(main, ends, tap):
-        first = jnp.where(row > 0, ends[0:1], 0.0)
-        last = jnp.where(row < n_row - 1, ends[1:2], 0.0)
-        at_row = index[:, : main.shape[1]]
-        before = jnp.where(at_row == 0, first, pltpu.roll(main, 1, 0))
-        after = jnp.where(at_row == rows - 1, last, pltpu.roll(main, rows - 1, 0))
-        return before * tap[0] + main * tap[1] + after * tap[2]
-
-    def rounded(value):
-        return value.astype(bf16).astype(f32)
-
-    other = 1 - lax.div(row, n_row // 2)
-    place = lax.rem(row, n_row // 2)
-    peers = [other * (n_row // 2) + lax.rem(place + i, n_row // 2) for i in range(n_row // 2)]
-    peers += [(1 - other) * (n_row // 2) + lax.rem(place + i, n_row // 2) for i in range(1, n_row // 2)]
-
-    sig_copies = []
-    for h in range(parts):
-        ends = rounded(dot(end_rows, weights[h]))
-        at = slice(h * wide, (h + 1) * wide)
+    def gs_share(j, value):
+        for p in range(n_col):
+            gs_send[p, j] = value[:, p * share : (p + 1) * share]
+        for o in range(1, n_col):
+            peer = lax.rem(col + o, n_col)
+            pltpu.make_async_remote_copy(
+                src_ref=gs_send.at[peer, j], dst_ref=gs_recv.at[col, j],
+                send_sem=gs_s.at[0], recv_sem=gs_r.at[0], device_id=(row, peer), device_id_type=mesh_id).start()
+        gs_recv[col, j] = gs_send[col, j]
+
+    for h in range(halves):
+        if h > 0:
+            arrived(weights.at[h], load_sem.at[3 + h])
+        main = rounded(halved(weights[h]))
+        if h == 0:
+            @pl.when(row > 0)
+            def _():
+                down.wait_recv()
+
+            @pl.when(row < n_row - 1)
+            def _():
+                up.wait_recv()
+
+            pl.semaphore_wait(alive.at[rounds - 1], either(known // 2))
+            for j in range(2):
+                edge_ref[j] = edge_in[j].astype(f32)
+                for i in range(depth // LANES):
+                    end_ref[j : j + 1, i * LANES : (i + 1) * LANES] = edge_ref[j, i : i + 1, :]
+            end_rows = end_ref[...].astype(bf16)
+        ends = rounded(edged(weights[h]))
+        at = slice(h * LANES, (h + 1) * LANES)
         tap = [jnp.concatenate([taps[i, 1:2, at], taps[i, 2:3, at]], 1) for i in range(3)]
-        made = convolved(proj_ref[h].astype(f32), ends, tap)
-        signal = (made[:, :wide] * made[:, wide:]).astype(bf16).astype(f32).T
+        made = convolved(main, ends, tap)
+        signal = (made[:, :LANES] * made[:, LANES:]).astype(bf16).astype(f32).T
         signal_ref[h] = signal
         flipped = signal.astype(bf16)
-        for g in range(n_row):
-            sig_send[h, g] = flipped[g * GROUP : (g + 1) * GROUP]
-        for i, peer in enumerate(peers):
-            sig_copies.append(pltpu.make_async_remote_copy(
-                src_ref=sig_send.at[h, peer], dst_ref=sig_recv.at[h, row],
-                send_sem=sig_s.at[h, i], recv_sem=sig_r.at[h, i],
-                device_id=(peer, col), device_id_type=mesh_id))
-            sig_copies[-1].start()
-        sig_recv[h, row] = sig_send[h, row]
-
+        for q in range(h * pair, (h + 1) * pair):
+            for g in range(n_row):
+                top = (q - h * pair) * wide + g * GROUP
+                sig_send[q, g] = flipped[top : top + GROUP]
+            for i, peer in enumerate(peers):
+                pltpu.make_async_remote_copy(
+                    src_ref=sig_send.at[q, peer], dst_ref=sig_recv.at[q, row],
+                    send_sem=sig_s.at[0], recv_sem=sig_r.at[q],
+                    device_id=(peer, col), device_id_type=mesh_id).start()
+            sig_recv[q, row] = sig_send[q, row]
+
+    skip_col = jnp.broadcast_to(skip[...], (LANES, width)).T
+    direct = jnp.concatenate([signal_ref[h] * skip_col[h * LANES : (h + 1) * LANES, 0:1] for h in range(halves)], 0)
+    gs_share(1, direct.astype(bf16))
+
+    hidden_chunk(pieces - 1)
+    to_partner[pieces - 1].start()
     outer_load.wait()
-    skip_col = jnp.broadcast_to(skip[...], (LANES, width)).T
-    for h in range(parts):
-        at = slice(h * wide, (h + 1) * wide)
-        main = rounded(dot(tok[...], outer_w[:, at]))
-        ends = rounded(dot(end_rows, outer_w[:, at]))
-        gate = rounded(convolved(main, ends, [taps[i, 0:1, at] for i in range(3)])).T.astype(bf16)
-        direct = (signal_ref[h] * skip_col[at, 0:1]).astype(bf16)
-        for p in range(n_col):
-            gs_send[p, 0, h] = gate[:, p * share : (p + 1) * share]
-            gs_send[p, 1, h] = direct[:, p * share : (p + 1) * share]
-    gs_copies = []
-    for o in range(1, n_col):
-        peer = lax.rem(col + o, n_col)
-        gs_copies.append(pltpu.make_async_remote_copy(
-            src_ref=gs_send.at[peer], dst_ref=gs_recv.at[col],
-            send_sem=gs_s.at[o], recv_sem=gs_r.at[o], device_id=(row, peer), device_id_type=mesh_id))
-        gs_copies[-1].start()
-    gs_recv[col] = gs_send[col]
-
-    for i in range(pieces // 2, pieces):
-        hidden_chunk(i)
-        to_partner[i].start()
+    main, ends = rounded(halved(outer_w[...])), rounded(edged(outer_w[...]))
+    gate = rounded(convolved(main, ends, [taps[i, 0:1] for i in range(3)])).T.astype(bf16)
+    gs_share(0, gate)
 
     def filter_chunk(owner, i):
         start = owner * half + i * CHUNK
@@ -574,8 +602,8 @@
 
     for i in range(pieces):
         filter_chunk(side, i)
+    arrived(hid.at[1 - side], hid_r.at[0])
     for i in range(pieces):
-        to_partner[i].wait_recv()
         filter_chunk(1 - side, i)
     scale_ref[...] = lax.rsqrt(1.0 + energy_ref[...]) * (0.5 / length)
 
@@ -607,10 +635,8 @@
     filt[0] = dot(turned[0], trig[:, :WIDE])
     filt[1] = dot(turned[1], trig[:, WIDE:])
 
-    resp_copies = []
     for h in range(parts):
-        for copy in sig_copies[h * (n_row - 1) : (h + 1) * (n_row - 1)]:
-            copy.wait_recv()
+        arrived(sig_recv.at[h, pl.ds(0, n_row - 1)], sig_r.at[h])
         band = pl.ds(h * spec, spec)
 
         def signal_tile(i, carry):
@@ -645,25 +671,19 @@
                 if i == n_row - 1 and o == 0:
                     continue
                 target = lax.rem(col + o, n_col)
-                resp_copies.append(pltpu.make_async_remote_copy(
+                pltpu.make_async_remote_copy(
                     src_ref=resp_send.at[h, peer, target], dst_ref=resp_recv.at[h, col, row],
-                    send_sem=resp_s.at[h], recv_sem=resp_r.at[h, col],
-                    device_id=(peer, target), device_id_type=mesh_id))
-                resp_copies[-1].start()
+                    send_sem=resp_s.at[0], recv_sem=resp_r.at[h],
+                    device_id=(peer, target), device_id_type=mesh_id).start()
         resp_recv[h, col, row] = resp_send[h, row, col]
 
-    for copy in gs_copies:
-        copy.wait_recv()
-    for copy in output_loads:
-        copy.wait()
+    arrived(gs_recv.at[pl.ds(0, n_col - 1)], gs_r.at[0])
+    arrived(output_w, load_sem.at[base + 1])
     for h in range(parts):
-        for o in range(n_col):
-            source = lax.rem(col + o, n_col)
-            come = resp_recv.at[h, source, pl.ds(0, n_row - 1 if o == 0 else n_row)]
-            pltpu.make_async_copy(come, come, resp_r.at[h, source]).wait()
+        arrived(resp_recv.at[h].reshape(n_row * n_col, GROUP, share).at[pl.ds(0, n_row * n_col - 1)], resp_r.at[h])
         shape = (n_col * wide, share)
         response = resp_recv[h].reshape(shape).astype(f32)
-        gate, direct = (gs_recv[:, j, h].reshape(shape).astype(f32) for j in range(2))
+        gate, direct = (gs_recv[:, j, h * wide : (h + 1) * wide].reshape(shape).astype(f32) for j in range(2))
         mixed = (gate * (response + direct)).T.astype(bf16)
         got = dot(mixed, output_w[h])
         if h == 0:
@@ -681,11 +701,10 @@
     def _():
         up.wait_send()
 
-    for copy in to_partner + sig_copies + gs_copies:
-        copy.wait_send()
-    for h in range(parts):
-        gone = resp_send.at[h].reshape(n_row * n_col, GROUP, share).at[pl.ds(0, n_row * n_col - 1)]
-        pltpu.make_async_copy(gone, gone, resp_s.at[h]).wait()
+    arrived(hid.at[side], hid_s.at[0])
+    arrived(sig_send.at[:, pl.ds(0, n_row - 1)], sig_s.at[0])
+    arrived(gs_send.at[pl.ds(0, n_col - 1)], gs_s.at[0])
+    arrived(resp_send.reshape(parts, n_row * n_col, GROUP, share).at[:, pl.ds(0, n_row * n_col - 1)], resp_s.at[0])
 
 
 def fits(tokens_rows, seq_length, own_width, row_devices, col_devices, units):
@@ -694,7 +713,10 @@
     return (
         members % (2 * GROUP) == 0
         and own_width % row_devices == 0
-        and row_devices * GROUP % LANES == 0
+        and LANES % (row_devices * GROUP) == 0
+        and own_width % LANES == 0
+        and row_devices <= REACH * 2 ** ROUNDS
+        and row_devices > REACH * 2 ** (ROUNDS - 1)
         and row_devices % 2 == 0
         and tokens_rows % WIDE == 0
         and planes % 8 == 0
@@ -718,6 +740,7 @@
     members = width // devices
     parts = members // GROUP
     wide = width // parts
+    halves = width // LANES
     planes = seq_length // WIDE
     n_col = lax.axis_size("col")
     k_index = np.arange(planes + 1)[:, None] * np.arange(WIDE)[None, :]
@@ -728,7 +751,6 @@
     trig = jnp.asarray(np.block([[cos_w, -sin_w], [sin_w, cos_w]]), bf16)
     spec = (planes + 1) * GROUP
     any_spec = pl.BlockSpec(memory_space=pl.ANY)
-    vmem = pl.BlockSpec(memory_space=pltpu.VMEM)
     dma = pltpu.SemaphoreType.DMA
     share = rows // n_col
     half = seq_length // 2
@@ -737,15 +759,15 @@
         conv_taps, feature_weight, feature_phase[None], inner_mats, inner_phase, frequency[None],
         forward_weight, backward_weight, decay_rate[None], skip_gain[None], twist, trig]
     exchanged = pltpu.VMEM((parts, devices, GROUP, rows), bf16)
-    spread = pltpu.VMEM((n_col, 2, parts, wide, share), bf16)
+    spread = pltpu.VMEM((n_col, 2, width, share), bf16)
     return pl.pallas_call(
         layer_kernel,
         out_shape=pltpu.VMEM((share, output_weight.shape[1]), bf16),
         in_specs=[any_spec] * (6 + len(small)),
-        out_specs=vmem,
+        out_specs=pl.BlockSpec(memory_space=pltpu.VMEM),
         scratch_shapes=[
             pltpu.VMEM((rows, depth), bf16),
-            pltpu.VMEM((parts, depth, 2 * wide), bf16),
+            pltpu.VMEM((halves, depth, 2 * LANES), bf16),
             pltpu.VMEM((depth, width), bf16),
             pltpu.VMEM((half, LANES), bf16),
             pltpu.VMEM((parts, n_col * wide, output_weight.shape[1]), bf16),
@@ -764,15 +786,15 @@
             pltpu.VMEM((2, width, LANES), f32),
             pltpu.VMEM((width, LANES), f32),
             pltpu.VMEM((members, LANES), f32),
-            pltpu.VMEM((parts, rows, 2 * wide), bf16),
-            pltpu.VMEM((parts, wide, rows), f32),
+            pltpu.VMEM((halves, LANES, rows), f32),
             pltpu.VMEM((share, output_weight.shape[1]), f32),
             pltpu.VMEM((2, depth // LANES, LANES), f32),
             pltpu.VMEM((2, depth // LANES, LANES), bf16),
             pltpu.VMEM((2, depth // LANES, LANES), bf16),
             pltpu.VMEM((16, depth), f32),
-            dma((5 + 2 * parts + parts * n_col,)), dma((len(small),)), dma((2,)), dma((2,)), dma((pieces,)), dma((pieces,)),
-            dma((parts, devices)), dma((parts, devices)), dma((n_col,)), dma((n_col,)), dma((parts,)), dma((parts, n_col)),
+            dma((5 + halves,)), dma((len(small),)), dma((2,)), dma((2,)), dma((1,)), dma((1,)),
+            dma((1,)), dma((parts,)), dma((1,)), dma((1,)), dma((1,)), dma((parts,)),
+            pltpu.SemaphoreType.REGULAR((ROUNDS,)),
         ],
         compiler_params=pltpu.CompilerParams(
             collective_id=0, has_side_effects=True, vmem_limit_bytes=GRANT),

time: 28.3 us -> 25.8 us (0.912)
  Pallas kernels: 27.4 us -> 24.8 us
    pallas_call x1, Pallas kernels: 27.4 us -> 24.8 us  [on_device_fast(): pl.pallas_call(layer_kernel, out_shape=pltpu.VMEM((share, output_weight.s...]
where the time goes in v2:
time: 25.8 us; the launch traced here: 25.6 us
  Pallas kernels  24.8 us (96%)
  local copies, waits for them, and re-layouts  0.8 us (3%)
    pallas_call x1, Pallas kernels, on_device_fast(): pl.pallas_call(layer_kernel, out_shape=pltpu.VMEM((share, output_weight.s...  24.8 us
    unnamed x1, local copies, waits for them, and re-layouts  0.8 us

profile of v2, /device:TPU:0, one launch (start us, length us, event | category | flops | bytes accessed | tf_op | source)
XLA Modules:
  0.0 25.6 jit_solution(10396856807898190787)
XLA Ops:
  0.0 24.8 %layer.1 = bf16[128,2048]{1,0:T(8,128)(2,1)S(1)} custom-call(bf16[512,2048]{1,0:T(8,128)(2,1)} %tokens_h.1, bf16[2048,256]{1,0:T(8,128)(2,1)} %outer_h.1, bf16[2048,256]{1,0:T(8,128)(2,1)} %inner_h.1, bf16[2048,256]{1,0:T(8,128)(2,1)} %value_h.1, bf16[4096,128]{1,0:T(8,128)(2,1)} %constant.8.clone.feats_h, bf16[1024,2048]{1,0:T(8,128)(2,1)} %output_h.1, ...), custom_call_target="tpu_custom_call" | custom-call | tf_op jit(solution)/shard_map/layer/pallas_call | solution.py:763
  24.8 0.8 %copy.20 = bf16[128,2048]{1,0:T(8,128)(2,1)} copy(bf16[128,2048]{1,0:T(8,128)(2,1)S(1)} %layer.1) | data formatting | bytes 1048576
